TPU v7x, 256 devices: a whole 4x4x8 slice. The times are simulated.
256 devices in a mesh: ra: 16 (over y, x), cb: 16 (over z, core).
Axes of the slice: x: 4, y: 4, z: 8, core: 2. Of those that a mesh axis runs over, the one named last changes fastest.
Arguments:
- tokens: bfloat16 [768, 4096], P(None, 'ra'), may hold values from -27 to 27, as said below
- gain_first: float32 [4096], P('ra'), may hold values from 0.1 to 1.9
- up_first: bfloat16 [4096, 16384], P('ra', 'cb'), may hold values from -0.09375 to 0.09375
- down_first: bfloat16 [16384, 4096], P('cb', 'ra'), may hold values from -0.046875 to 0.046875
- gain_second: float32 [4096], P('ra'), may hold values from 0.1 to 1.9
- up_second: bfloat16 [4096, 16384], P('ra', 'cb'), may hold values from -0.09375 to 0.09375
- down_second: bfloat16 [16384, 4096], P('cb', 'ra'), may hold values from -0.046875 to 0.046875
Outputs:
- mixed: bfloat16 [768, 4096], P(None, 'ra')
Inputs may be any that keep to these rules, and one draw needn't show every extreme that they name: `tokens`: channels come in 32 groups of equal width with different scales.
All inputs are finite; a program needn't handle non-finite values.
Results may differ from a plain program's by a relative error of at most 0.0079.
Values may be sent and summed in bfloat16 or wider, within the bound.
No kernel may reach another device: no remote copies, remote signals or barrier semaphores. Data moves between devices by JAX's collectives and lax.ppermute only.
A program may use at most 64 MiB of HBM per device.

v0:
```python
import jax
import jax.numpy as jnp
from jax import lax
from jax.sharding import PartitionSpec as P


def split_up(x, dim, peers):
    before, after = (x.shape[:dim], x.shape[dim + 1 :])
    return jnp.moveaxis(x.reshape(*before, peers, -1, *after), dim, 0)


def summed_on_arrival(x, axis, dim):
    peers = lax.axis_size(axis)
    parts = lax.all_to_all(split_up(x, dim, peers), axis, 0, 0, tiled=True)
    return jnp.sum(parts, axis=0)


def laid_out(parts, dim):
    shape = list(parts.shape[1:])
    shape[dim] *= parts.shape[0]
    return jnp.moveaxis(parts, 0, dim).reshape(shape)


def copy_for_each(x, axis):
    peers = lax.axis_size(axis)
    return lax.all_to_all(jnp.broadcast_to(x[None], (peers, *x.shape)), axis, 0, 0, tiled=True)


def collect(x, axis, dim):
    return laid_out(copy_for_each(x, axis), dim)


def sublayer(x, gain, w_up, w_down):
    xf = x.astype(jnp.float32)
    groups = lax.axis_size("ra")
    width = x.shape[1] * groups
    partial_sq = jnp.sum(xf * xf, axis=1)
    scaled = (xf * gain[None, :]).astype(jnp.bfloat16)
    partial_value = jnp.dot(scaled, w_up, preferred_element_type=jnp.float32)
    tiled_sq = jnp.broadcast_to(partial_sq[:, None], (x.shape[0], groups))
    share, total_tile = (
        summed_on_arrival(partial_value, "ra", 1),
        summed_on_arrival(tiled_sq, "ra", 1),
    )
    factor = lax.rsqrt(total_tile[:, 0] / width + 1e-06)
    act = jax.nn.relu(share * factor[:, None])
    hidden_share = (act * act).astype(jnp.bfloat16)
    local_out = jnp.dot(collect(hidden_share, "ra", 1), w_down, preferred_element_type=jnp.float32)
    branch_rows = summed_on_arrival(local_out, "cb", 0)
    count = branch_rows.shape[0]
    offset = lax.axis_index("cb") * count
    own = lax.dynamic_slice_in_dim(xf, offset, count, 0)
    finished = (0.5 * own + branch_rows).astype(jnp.bfloat16)
    return collect(finished, "cb", 0)


def body(tokens, gain_first, up_first, down_first, gain_second, up_second, down_second):
    middle = sublayer(tokens, gain_first, up_first, down_first)
    return sublayer(middle, gain_second, up_second, down_second)


def solution(mesh):
    placed = (
        P(None, "ra"),
        P("ra"),
        P("ra", "cb"),
        P("cb", "ra"),
        P("ra"),
        P("ra", "cb"),
        P("cb", "ra"),
    )
    return jax.shard_map(body, mesh=mesh, in_specs=placed, out_specs=P(None, "ra"), check_vma=False)
```

profile of v0, /device:TPU:1, one launch (start us, length us, event | category | flops | bytes accessed | tf_op | source)
XLA Modules:
  0.0 301.3 jit_solution(7780635838265782067)
XLA Ops:
  1.9 7.6 %all-to-all-start.1 = ((f32[16,768,1]{1,2,0:T(1,128)}), f32[16,768,1]{1,2,0:T(1,128)S(1)}, u32[]{:S(2)}, u32[]{:S(2)}) async-start(f32[16,768,1]{1,2,0:T(1,128)} %transpose.30), calls=%async_computation.1 | async-start | bytes 98304 | tf_op jit(solution)/shard_map/all_to_all | solution.py:14
  9.5 3.3 %fusion.4 = f32[768,1024]{0,1:T(8,128)} fusion(bf16[256,1024]{1,0:T(8,128)(2,1)S(1)} %copy-done, f32[256]{0:T(256)} %param.8, bf16[768,256]{1,0:T(8,128)(2,1)} %param.7), kind=kOutput, calls=%fused_computation.9 | convolution fusion | flops 403243008 | bytes 4064256 | tf_op jit(solution)/shard_map/dot_general | solution.py:39
  12.8 3.1 %all-to-all-done.1 = f32[16,768,1]{1,2,0:T(1,128)S(1)} async-done(((f32[16,768,1]{1,2,0:T(1,128)}), f32[16,768,1]{1,2,0:T(1,128)S(1)}, u32[]{:S(2)}, u32[]{:S(2)}) %all-to-all-start.1) | async-done | bytes 49184 | tf_op jit(solution)/shard_map/all_to_all | solution.py:14
  16.0 4.5 %all-to-all-start = ((f32[16,768,64]{1,2,0:T(8,128)}), f32[16,768,64]{1,2,0:T(8,128)}, u32[]{:S(2)}, u32[]{:S(2)}) async-start(f32[16,768,64]{1,2,0:T(8,128)} %bitcast.28), calls=%async_computation | async-start | bytes 6291456 | tf_op jit(solution)/shard_map/all_to_all | solution.py:14
  20.5 43.1 %all-to-all-done = f32[16,768,64]{1,2,0:T(8,128)} async-done(((f32[16,768,64]{1,2,0:T(8,128)}), f32[16,768,64]{1,2,0:T(8,128)}, u32[]{:S(2)}, u32[]{:S(2)}) %all-to-all-start) | async-done | bytes 3145760 | tf_op jit(solution)/shard_map/all_to_all | solution.py:14
  63.6 2.1 reduce_sum.72
  65.8 25.6 %all_to_all.50 = bf16[16,768,64]{1,2,0:T(8,128)(2,1)S(1)} all-to-all(bf16[16,768,64]{1,2,0:T(8,128)(2,1)S(1)} %broadcast_in_dim.10), channel_id=1, replica_groups=mesh['ra'=16,'cb'=16] {'ra'}, dimensions={0} | all-to-all | bytes 3145728 | tf_op jit(solution)/shard_map/all_to_all | solution.py:26
  91.4 3.8 %copy.12 = bf16[768,16,64]{2,1,0:T(8,128)(2,1)} copy(bf16[768,16,64]{0,2,1:T(8,128)(2,1)S(1)} %bitcast.29) | data formatting | bytes 3145728 | tf_op jit(solution)/shard_map/transpose | solution.py:21
  95.2 4.5 %dot_general.21 = bf16[16,48,1024]{2,1,0:T(8,128)(2,1)S(1)} reshape(bf16[768,16,64]{2,1,0:T(8,128)(2,1)} %copy.12) | data formatting | bytes 3145728 | tf_op jit(solution)/shard_map/dot_general | solution.py:48
  101.2 11.3 %all-to-all-start.3 = ((f32[16,48,256]{2,1,0:T(8,128)}), f32[16,48,256]{2,1,0:T(8,128)S(1)}, u32[]{:S(2)}, u32[]{:S(2)}) async-start(f32[16,48,256]{2,1,0:T(8,128)} %fusion.2), calls=%async_computation.3 | async-start | bytes 1572864 | tf_op jit(solution)/shard_map/all_to_all | solution.py:14
  112.6 22.6 %all-to-all-done.3 = f32[16,48,256]{2,1,0:T(8,128)S(1)} async-done(((f32[16,48,256]{2,1,0:T(8,128)}), f32[16,48,256]{2,1,0:T(8,128)S(1)}, u32[]{:S(2)}, u32[]{:S(2)}) %all-to-all-start.3) | async-done | bytes 786464 | tf_op jit(solution)/shard_map/all_to_all | solution.py:14
  136.1 3.5 %all-to-all-start.4 = ((bf16[16,48,256]{2,1,0:T(8,128)(2,1)}), bf16[16,48,256]{2,1,0:T(8,128)(2,1)S(1)}, u32[]{:S(2)}, u32[]{:S(2)}) async-start(bf16[16,48,256]{2,1,0:T(8,128)(2,1)} %broadcast_in_dim.11), calls=%async_computation.4 | async-start | bytes 786432 | tf_op jit(solution)/shard_map/all_to_all | solution.py:26
  139.8 13.8 %all-to-all-done.4 = bf16[16,48,256]{2,1,0:T(8,128)(2,1)S(1)} async-done(((bf16[16,48,256]{2,1,0:T(8,128)(2,1)}), bf16[16,48,256]{2,1,0:T(8,128)(2,1)S(1)}, u32[]{:S(2)}, u32[]{:S(2)}) %all-to-all-start.4) | async-done | bytes 393248 | tf_op jit(solution)/shard_map/all_to_all | solution.py:26
  154.5 3.5 %all-to-all-start.6 = ((f32[16,768,1]{1,2,0:T(1,128)}), f32[16,768,1]{1,2,0:T(1,128)S(1)}, u32[]{:S(2)}, u32[]{:S(2)}) async-start(f32[16,768,1]{1,2,0:T(1,128)} %transpose.33), calls=%async_computation.6 | async-start | bytes 98304 | tf_op jit(solution)/shard_map/all_to_all | solution.py:14
  158.0 2.3 convolution_bitcast_fusion
  160.3 4.5 %all-to-all-done.6 = f32[16,768,1]{1,2,0:T(1,128)S(1)} async-done(((f32[16,768,1]{1,2,0:T(1,128)}), f32[16,768,1]{1,2,0:T(1,128)S(1)}, u32[]{:S(2)}, u32[]{:S(2)}) %all-to-all-start.6) | async-done | bytes 49184 | tf_op jit(solution)/shard_map/all_to_all | solution.py:14
  164.8 4.5 %all-to-all-start.5 = ((f32[16,768,64]{1,2,0:T(8,128)}), f32[16,768,64]{1,2,0:T(8,128)}, u32[]{:S(2)}, u32[]{:S(2)}) async-start(f32[16,768,64]{1,2,0:T(8,128)} %convolution_bitcast_fusion), calls=%async_computation.5 | async-start | bytes 6291456 | tf_op jit(solution)/shard_map/all_to_all | solution.py:14
  169.3 47.7 %all-to-all-done.5 = f32[16,768,64]{1,2,0:T(8,128)} async-done(((f32[16,768,64]{1,2,0:T(8,128)}), f32[16,768,64]{1,2,0:T(8,128)}, u32[]{:S(2)}, u32[]{:S(2)}) %all-to-all-start.5) | async-done | bytes 3145760 | tf_op jit(solution)/shard_map/all_to_all | solution.py:14
  219.3 25.4 %all_to_all.51 = bf16[16,768,64]{1,2,0:T(8,128)(2,1)S(1)} all-to-all(bf16[16,768,64]{1,2,0:T(8,128)(2,1)S(1)} %broadcast_in_dim.13), channel_id=1, replica_groups=mesh['ra'=16,'cb'=16] {'ra'}, dimensions={0} | all-to-all | bytes 3145728 | tf_op jit(solution)/shard_map/all_to_all | solution.py:26
  244.7 3.8 %copy.14 = bf16[768,16,64]{2,1,0:T(8,128)(2,1)} copy(bf16[768,16,64]{0,2,1:T(8,128)(2,1)S(1)} %bitcast.30) | data formatting | bytes 3145728 | tf_op jit(solution)/shard_map/transpose | solution.py:21
  248.5 4.5 %dot_general.26 = bf16[16,48,1024]{2,1,0:T(8,128)(2,1)S(1)} reshape(bf16[768,16,64]{2,1,0:T(8,128)(2,1)} %copy.14) | data formatting | bytes 3145728 | tf_op jit(solution)/shard_map/dot_general | solution.py:48
  254.5 5.8 %all-to-all-start.8 = ((f32[16,48,256]{2,1,0:T(8,128)}), f32[16,48,256]{2,1,0:T(8,128)S(1)}, u32[]{:S(2)}, u32[]{:S(2)}) async-start(f32[16,48,256]{2,1,0:T(8,128)} %fusion), calls=%async_computation.8 | async-start | bytes 1572864 | tf_op jit(solution)/shard_map/all_to_all | solution.py:14
  260.4 22.7 %all-to-all-done.8 = f32[16,48,256]{2,1,0:T(8,128)S(1)} async-done(((f32[16,48,256]{2,1,0:T(8,128)}), f32[16,48,256]{2,1,0:T(8,128)S(1)}, u32[]{:S(2)}, u32[]{:S(2)}) %all-to-all-start.8) | async-done | bytes 786464 | tf_op jit(solution)/shard_map/all_to_all | solution.py:14
  283.2 17.4 %all_to_all.52 = bf16[16,48,256]{2,1,0:T(8,128)(2,1)S(1)} all-to-all(bf16[16,48,256]{2,1,0:T(8,128)(2,1)S(1)} %broadcast_in_dim.14), channel_id=1, replica_groups=mesh['ra'=16,'cb'=16] {'cb'}, dimensions={0} | all-to-all | bytes 786432 | tf_op jit(solution)/shard_map/all_to_all | solution.py:26
  (38 shorter events, 10.3 us)
Async XLA Ops:
  0.0 9.5 %copy-start = (bf16[256,1024]{1,0:T(8,128)(2,1)S(1)}, bf16[256,1024]{1,0:T(8,128)(2,1)}, u32[]{:S(2)}) copy-start(bf16[256,1024]{1,0:T(8,128)(2,1)} %param.9) | copy-start | bytes 1572868
  1.9 14.1 %all-to-all-start.1 = ((f32[16,768,1]{1,2,0:T(1,128)}), f32[16,768,1]{1,2,0:T(1,128)S(1)}, u32[]{:S(2)}, u32[]{:S(2)}) async-start(f32[16,768,1]{1,2,0:T(1,128)} %transpose.30), calls=%async_computation.1 | async-start | bytes 98304 | tf_op jit(solution)/shard_map/all_to_all | solution.py:14
  16.0 47.6 %all-to-all-start = ((f32[16,768,64]{1,2,0:T(8,128)}), f32[16,768,64]{1,2,0:T(8,128)}, u32[]{:S(2)}, u32[]{:S(2)}) async-start(f32[16,768,64]{1,2,0:T(8,128)} %bitcast.28), calls=%async_computation | async-start | bytes 6291456 | tf_op jit(solution)/shard_map/all_to_all | solution.py:14
  95.2 4.5 %copy-start.3 = (bf16[1024,256]{1,0:T(8,128)(2,1)S(1)}, bf16[1024,256]{1,0:T(8,128)(2,1)}, u32[]{:S(2)}) copy-start(bf16[1024,256]{1,0:T(8,128)(2,1)} %param.10) | copy-start | bytes 1572868
  99.8 12.8 %copy-start.1 = (bf16[768,256]{1,0:T(8,128)(2,1)S(1)}, bf16[768,256]{1,0:T(8,128)(2,1)}, u32[]{:S(2)}) copy-start(bf16[768,256]{1,0:T(8,128)(2,1)} %param.7) | copy-start | bytes 1179652
  101.2 34.0 %all-to-all-start.3 = ((f32[16,48,256]{2,1,0:T(8,128)}), f32[16,48,256]{2,1,0:T(8,128)S(1)}, u32[]{:S(2)}, u32[]{:S(2)}) async-start(f32[16,48,256]{2,1,0:T(8,128)} %fusion.2), calls=%async_computation.3 | async-start | bytes 1572864 | tf_op jit(solution)/shard_map/all_to_all | solution.py:14
  112.5 27.0 %copy-start.2 = (bf16[256,1024]{1,0:T(8,128)(2,1)S(1)}, bf16[256,1024]{1,0:T(8,128)(2,1)}, u32[]{:S(2)}) copy-start(bf16[256,1024]{1,0:T(8,128)(2,1)} %param.12) | copy-start | bytes 1572868
  112.6 40.9 %copy-start.5 = (f32[256]{0:T(256)S(1)}, f32[256]{0:T(256)}, u32[]{:S(2)}) copy-start(f32[256]{0:T(256)} %param.11) | copy-start | bytes 3076
  136.1 17.5 %all-to-all-start.4 = ((bf16[16,48,256]{2,1,0:T(8,128)(2,1)}), bf16[16,48,256]{2,1,0:T(8,128)(2,1)S(1)}, u32[]{:S(2)}, u32[]{:S(2)}) async-start(bf16[16,48,256]{2,1,0:T(8,128)(2,1)} %broadcast_in_dim.11), calls=%async_computation.4 | async-start | bytes 786432 | tf_op jit(solution)/shard_map/all_to_all | solution.py:26
  154.5 10.3 %all-to-all-start.6 = ((f32[16,768,1]{1,2,0:T(1,128)}), f32[16,768,1]{1,2,0:T(1,128)S(1)}, u32[]{:S(2)}, u32[]{:S(2)}) async-start(f32[16,768,1]{1,2,0:T(1,128)} %transpose.33), calls=%async_computation.6 | async-start | bytes 98304 | tf_op jit(solution)/shard_map/all_to_all | solution.py:14
  164.8 52.3 %all-to-all-start.5 = ((f32[16,768,64]{1,2,0:T(8,128)}), f32[16,768,64]{1,2,0:T(8,128)}, u32[]{:S(2)}, u32[]{:S(2)}) async-start(f32[16,768,64]{1,2,0:T(8,128)} %convolution_bitcast_fusion), calls=%async_computation.5 | async-start | bytes 6291456 | tf_op jit(solution)/shard_map/all_to_all | solution.py:14
  248.5 4.5 %copy-start.4 = (bf16[1024,256]{1,0:T(8,128)(2,1)S(1)}, bf16[1024,256]{1,0:T(8,128)(2,1)}, u32[]{:S(2)}) copy-start(bf16[1024,256]{1,0:T(8,128)(2,1)} %param.13) | copy-start | bytes 1572868
  254.5 28.6 %all-to-all-start.8 = ((f32[16,48,256]{2,1,0:T(8,128)}), f32[16,48,256]{2,1,0:T(8,128)S(1)}, u32[]{:S(2)}, u32[]{:S(2)}) async-start(f32[16,48,256]{2,1,0:T(8,128)} %fusion), calls=%async_computation.8 | async-start | bytes 1572864 | tf_op jit(solution)/shard_map/all_to_all | solution.py:14
where the time goes:
time: 302 us; the launch traced here: 301 us
  waiting for transfers between devices  158 us (52%)
  blocking collectives  68.3 us (23%)
  starting transfers between devices  40.5 us (13%)
  local copies, waits for them, and re-layouts  20.1 us (7%)
  matrix products  8.56 us (3%)
  other arithmetic  5.95 us (2%)
    all_to_all x6, waiting for transfers between devices, summed_on_arrival(): parts = lax.all_to_all(split_up(x, dim, peers), axis, 0, 0, tiled=True)  144 us
    all_to_all x3, blocking collectives, copy_for_each(): lax.all_to_all(jnp.broadcast_to(x[None], (peers, *x.shape)), axis, 0, 0,...  68.3 us
    all_to_all x6, starting transfers between devices, summed_on_arrival(): parts = lax.all_to_all(split_up(x, dim, peers), axis, 0, 0, tiled=True)  37.1 us
    all_to_all x1, waiting for transfers between devices, copy_for_each(): lax.all_to_all(jnp.broadcast_to(x[None], (peers, *x.shape)), axis, 0, 0,...  13.8 us
    dot_general x2, local copies, waits for them, and re-layouts, sublayer(): jnp.dot(collect(hidden_share, 'ra', 1), w_down, preferred_element_type=jn...  9.05 us
    transpose x2, local copies, waits for them, and re-layouts, laid_out(): return jnp.moveaxis(parts, 0, dim).reshape(shape)  7.64 us
  transfers between devices with their start and end apart: 7, of which 7 were waited for; matrix products, arithmetic and copies ran while one was open for 2% of the time, Pallas kernels for 0%

commit v1 on v0

v1 whole, which is shorter than its diff:
```python
import jax
import jax.numpy as jnp
from jax import lax
from jax.sharding import Mesh, PartitionSpec as P

RA = ("y", "x")
BF = jnp.bfloat16
F32 = jnp.float32


def exchange(parts, axis):
    return lax.all_to_all(parts, axis, 0, 0, tiled=True)


def copy_for_each(x, axis):
    peers = lax.axis_size(axis)
    return exchange(jnp.broadcast_to(x[None], (peers, *x.shape)), axis)


def from_other_core(w):
    return lax.ppermute(w, "c", [(0, 1), (1, 0)])


def sublayer(x, gain, up_own, up_other, down_own, down_other, width):
    tokens, _ = x.shape
    peers = lax.axis_size(RA)
    xf = x.astype(F32)
    sq = jnp.sum(xf * xf, axis=1, keepdims=True)
    high = sq.astype(BF)
    low = (sq - high.astype(F32)).astype(BF)
    scaled = (xf * gain[None, :]).astype(BF)
    up = jnp.concatenate([up_own, up_other], axis=1)
    hidden_width = up.shape[1]
    pre = jnp.dot(scaled, up, preferred_element_type=F32).astype(BF)
    stats = jnp.concatenate([high, low, jnp.zeros((tokens, 126), BF)], axis=1)
    payload = jnp.concatenate([pre, stats], axis=1).reshape(peers, tokens // peers, -1)
    total = jnp.sum(exchange(payload, RA).astype(F32), axis=0)
    meansq = (total[:, hidden_width] + total[:, hidden_width + 1]) / width
    act = jax.nn.relu(total[:, :hidden_width] * lax.rsqrt(meansq + 1e-06)[:, None])
    hidden = copy_for_each((act * act).astype(BF), RA).reshape(tokens, hidden_width)
    down = jnp.concatenate([down_own, down_other], axis=0)
    branch = jnp.dot(hidden, down, preferred_element_type=F32).astype(BF)
    planes = lax.axis_size("z")
    count = tokens // planes
    rows = jnp.sum(exchange(branch.reshape(planes, count, -1), "z").astype(F32), axis=0)
    own = lax.dynamic_slice_in_dim(xf, lax.axis_index("z") * count, count, 0)
    finished = (0.5 * own + rows).astype(BF)
    return copy_for_each(finished, "z").reshape(tokens, -1)


def body(tokens, gain_first, up_first, down_first, gain_second, up_second, down_second):
    width = tokens.shape[1] * lax.axis_size(RA)
    half = tokens.shape[0] // 2
    core = lax.axis_index("c")
    x = lax.dynamic_slice_in_dim(tokens, core * half, half, 0)
    others = [from_other_core(w) for w in (up_first, down_first, up_second, down_second)]
    x = sublayer(x, gain_first, up_first, others[0], down_first, others[1], width)
    x = sublayer(x, gain_second, up_second, others[2], down_second, others[3], width)
    y = from_other_core(x)
    first = core == 0
    return jnp.concatenate([jnp.where(first, x, y), jnp.where(first, y, x)], axis=0)


def solution(mesh):
    fine = Mesh(mesh.devices.reshape(4, 4, 8, 2), ("y", "x", "z", "c"))
    cb = ("z", "c")
    placed = (
        P(None, RA),
        P(RA),
        P(RA, cb),
        P(cb, RA),
        P(RA),
        P(RA, cb),
        P(cb, RA),
    )
    return jax.shard_map(body, mesh=fine, in_specs=placed, out_specs=P(None, RA), check_vma=False)
```

time: 302 us -> 181 us (0.60)
  waiting for transfers between devices: 158 us -> 45.8 us
  local copies, waits for them, and re-layouts: 20.1 us -> 5.64 us
  blocking collectives: 68.3 us -> 76.6 us
  matrix products: 8.56 us -> 4.15 us
  starting transfers between devices: 40.5 us -> 43.7 us
    all_to_all x7 -> x4, waiting for transfers between devices: 158 us -> 41.4 us  [exchange(): return lax.all_to_all(parts, axis, 0, 0, tiled=True)]
    ppermute x0 -> x5, starting transfers between devices: none -> 24.3 us  [from_other_core(): return lax.ppermute(w, 'c', [(0, 1), (1, 0)])]
    all_to_all x7 -> x4, starting transfers between devices: 40.5 us -> 19.4 us  [exchange(): return lax.all_to_all(parts, axis, 0, 0, tiled=True)]
    dot_general x2 -> x0, local copies, waits for them, and re-layouts: 9.05 us -> none  [sublayer(): jnp.dot(collect(hidden_share, 'ra', 1), w_down, preferred_element_type=jn...]
    transpose x4 -> x0, local copies, waits for them, and re-layouts: 8.94 us -> none  [the longest x2 7.64 us: laid_out(): return jnp.moveaxis(parts, 0, dim).reshape(shape)]
    all_to_all x3 -> x4, blocking collectives: 68.3 us -> 76.6 us  [exchange(): return lax.all_to_all(parts, axis, 0, 0, tiled=True)]
    dot_general x4, matrix products: 8.56 us -> 4.15 us  [the longest x2 2.32 us: sublayer(): pre = jnp.dot(scaled, up, preferred_element_type=F32).astype(BF)]
    ppermute x0 -> x5, waiting for transfers between devices: none -> 4.33 us  [from_other_core(): return lax.ppermute(w, 'c', [(0, 1), (1, 0)])]
  transfers between devices with their start and end apart: 7 -> 9, of which waited for: 7 -> 8; matrix products, arithmetic and copies ran while one was open for 2% -> 1% of each run, Pallas kernels for 0% -> 0%
where the time goes in v1:
time: 181 us; the launch traced here: 180 us
  blocking collectives  76.6 us (42%)
  waiting for transfers between devices  45.8 us (25%)
  starting transfers between devices  43.7 us (24%)
  local copies, waits for them, and re-layouts  5.64 us (3%)
  matrix products  4.15 us (2%)
  other arithmetic  4.02 us (2%)
    all_to_all x4, blocking collectives, exchange(): return lax.all_to_all(parts, axis, 0, 0, tiled=True)  76.6 us
    all_to_all x4, waiting for transfers between devices, exchange(): return lax.all_to_all(parts, axis, 0, 0, tiled=True)  41.4 us
    ppermute x5, starting transfers between devices, from_other_core(): return lax.ppermute(w, 'c', [(0, 1), (1, 0)])  24.3 us
    all_to_all x4, starting transfers between devices, exchange(): return lax.all_to_all(parts, axis, 0, 0, tiled=True)  19.4 us
    ppermute x5, waiting for transfers between devices, from_other_core(): return lax.ppermute(w, 'c', [(0, 1), (1, 0)])  4.33 us
  transfers between devices with their start and end apart: 9, of which 8 were waited for; matrix products, arithmetic and copies ran while one was open for 1% of the time, Pallas kernels for 0%

profile of v1, /device:TPU:1, one launch (start us, length us, event | category | flops | bytes accessed | tf_op | source)
XLA Modules:
  0.0 180.1 jit_solution(12351118052100241945)
XLA Ops:
  0.0 3.2 %collective-permute-start = (bf16[256,1024]{1,0:T(8,128)(2,1)}, bf16[256,1024]{1,0:T(8,128)(2,1)S(1)}, u32[]{:S(2)}, u32[]{:S(2)}) collective-permute-start(bf16[256,1024]{1,0:T(8,128)(2,1)} %param.9), channel_id=1, source_target_pairs={{0,1},{1,0},{2,3},{3,2},{4,5},{5,4},{6,7},{7,6},{8,9},{9,8},{10,11... | collective-permute-start | bytes 1572872 | tf_op jit(solution)/shard_map/ppermute | solution.py:21
  3.2 1.1 multiply_reduce_fusion.1
  4.9 1.7 convolution_convert_fusion.1
  7.3 27.9 %all_to_all.40 = bf16[16,24,2176]{2,1,0:T(8,128)(2,1)S(1)} all-to-all(bf16[16,24,2176]{2,1,0:T(8,128)(2,1)S(1)} %concatenate.32), channel_id=1, replica_groups=mesh['y'=4,'x'=4,'z'=8,'c'=2] {'y','x'}, dimensions={0} | all-to-all | bytes 3342336 | tf_op jit(solution)/shard_map/all_to_all | solution.py:12
  35.7 1.3 broadcast_in_dim.8
  37.1 3.9 %all-to-all-start.1 = ((bf16[16,24,2048]{2,1,0:T(8,128)(2,1)}), bf16[16,24,2048]{2,1,0:T(8,128)(2,1)S(1)}, u32[]{:S(2)}, u32[]{:S(2)}) async-start(bf16[16,24,2048]{2,1,0:T(8,128)(2,1)} %broadcast_in_dim.8), calls=%async_computation.1 | async-start | bytes 3145728 | tf_op jit(solution)/shard_map/all_to_all | solution.py:12
  40.9 1.8 %collective-permute-start.1 = (bf16[1024,256]{1,0:T(8,128)(2,1)S(1)}, bf16[1024,256]{1,0:T(8,128)(2,1)S(1)}, u32[]{:S(2)}, u32[]{:S(2)}) collective-permute-start(bf16[1024,256]{1,0:T(8,128)(2,1)S(1)} %copy-done.4), channel_id=1, source_target_pairs={{0,1},{1,0},{2,3},{3,2},{4,5},{5,4},{6,7},{7,6},{8,9},{9,8},{10,11... | collective-permute-start | bytes 1572872 | tf_op jit(solution)/shard_map/ppermute | solution.py:21
  42.8 1.5 collective-permute-done.1
  44.3 17.5 %all-to-all-done.1 = bf16[16,24,2048]{2,1,0:T(8,128)(2,1)S(1)} async-done(((bf16[16,24,2048]{2,1,0:T(8,128)(2,1)}), bf16[16,24,2048]{2,1,0:T(8,128)(2,1)S(1)}, u32[]{:S(2)}, u32[]{:S(2)}) %all-to-all-start.1) | async-done | bytes 1572896 | tf_op jit(solution)/shard_map/all_to_all | solution.py:12
  61.8 1.3 convolution_convert_fusion.3
  63.1 8.3 %all-to-all-start.2 = ((bf16[8,48,256]{2,1,0:T(8,128)(2,1)}), bf16[8,48,256]{2,1,0:T(8,128)(2,1)S(1)}, u32[]{:S(2)}, u32[]{:S(2)}) async-start(bf16[8,48,256]{2,1,0:T(8,128)(2,1)} %bitcast.2), calls=%async_computation.2 | async-start | bytes 393216 | tf_op jit(solution)/shard_map/all_to_all | solution.py:12
  71.4 8.6 %all-to-all-done.2 = bf16[8,48,256]{2,1,0:T(8,128)(2,1)S(1)} async-done(((bf16[8,48,256]{2,1,0:T(8,128)(2,1)}), bf16[8,48,256]{2,1,0:T(8,128)(2,1)S(1)}, u32[]{:S(2)}, u32[]{:S(2)}) %all-to-all-start.2) | async-done | bytes 196640 | tf_op jit(solution)/shard_map/all_to_all | solution.py:12
  80.8 3.4 %all-to-all-start.3 = ((bf16[8,48,256]{2,1,0:T(8,128)(2,1)}), bf16[8,48,256]{2,1,0:T(8,128)(2,1)S(1)}, u32[]{:S(2)}, u32[]{:S(2)}) async-start(bf16[8,48,256]{2,1,0:T(8,128)(2,1)} %broadcast_in_dim.9), calls=%async_computation.3 | async-start | bytes 393216 | tf_op jit(solution)/shard_map/all_to_all | solution.py:12
  84.2 5.4 %collective-permute-start.2 = (bf16[256,1024]{1,0:T(8,128)(2,1)S(1)}, bf16[256,1024]{1,0:T(8,128)(2,1)S(1)}, u32[]{:S(2)}, u32[]{:S(2)}) collective-permute-start(bf16[256,1024]{1,0:T(8,128)(2,1)S(1)} %copy-done.1), channel_id=1, source_target_pairs={{0,1},{1,0},{2,3},{3,2},{4,5},{5,4},{6,7},{7,6},{8,9},{9,8},{10,11... | collective-permute-start | bytes 1572872 | tf_op jit(solution)/shard_map/ppermute | solution.py:21
  89.6 3.1 %all-to-all-done.3 = bf16[8,48,256]{2,1,0:T(8,128)(2,1)S(1)} async-done(((bf16[8,48,256]{2,1,0:T(8,128)(2,1)}), bf16[8,48,256]{2,1,0:T(8,128)(2,1)S(1)}, u32[]{:S(2)}, u32[]{:S(2)}) %all-to-all-start.3) | async-done | bytes 196640 | tf_op jit(solution)/shard_map/all_to_all | solution.py:12
  94.7 26.6 %all_to_all.41 = bf16[16,24,2176]{2,1,0:T(8,128)(2,1)S(1)} all-to-all(bf16[16,24,2176]{2,1,0:T(8,128)(2,1)S(1)} %concatenate.36), channel_id=1, replica_groups=mesh['y'=4,'x'=4,'z'=8,'c'=2] {'y','x'}, dimensions={0} | all-to-all | bytes 3342336 | tf_op jit(solution)/shard_map/all_to_all | solution.py:12
  121.9 1.3 broadcast_in_dim.10
  123.2 3.8 %all-to-all-start.5 = ((bf16[16,24,2048]{2,1,0:T(8,128)(2,1)}), bf16[16,24,2048]{2,1,0:T(8,128)(2,1)S(1)}, u32[]{:S(2)}, u32[]{:S(2)}) async-start(bf16[16,24,2048]{2,1,0:T(8,128)(2,1)} %broadcast_in_dim.10), calls=%async_computation.5 | async-start | bytes 3145728 | tf_op jit(solution)/shard_map/all_to_all | solution.py:12
  127.1 4.8 %collective-permute-start.3 = (bf16[1024,256]{1,0:T(8,128)(2,1)S(1)}, bf16[1024,256]{1,0:T(8,128)(2,1)S(1)}, u32[]{:S(2)}, u32[]{:S(2)}) collective-permute-start(bf16[1024,256]{1,0:T(8,128)(2,1)S(1)} %copy-done.5), channel_id=1, source_target_pairs={{0,1},{1,0},{2,3},{3,2},{4,5},{5,4},{6,7},{7,6},{8,9},{9,8},{10,11... | collective-permute-start | bytes 1572872 | tf_op jit(solution)/shard_map/ppermute | solution.py:21
  131.9 1.5 collective-permute-done.3
  133.4 12.2 %all-to-all-done.5 = bf16[16,24,2048]{2,1,0:T(8,128)(2,1)S(1)} async-done(((bf16[16,24,2048]{2,1,0:T(8,128)(2,1)}), bf16[16,24,2048]{2,1,0:T(8,128)(2,1)S(1)}, u32[]{:S(2)}, u32[]{:S(2)}) %all-to-all-start.5) | async-done | bytes 1572896 | tf_op jit(solution)/shard_map/all_to_all | solution.py:12
  146.2 11.0 %all_to_all.42 = bf16[8,48,256]{2,1,0:T(8,128)(2,1)S(1)} all-to-all(bf16[8,48,256]{2,1,0:T(8,128)(2,1)S(1)} %bitcast.19), channel_id=1, replica_groups=mesh['y'=4,'x'=4,'z'=8,'c'=2] {'z'}, dimensions={0} | all-to-all | bytes 393216 | tf_op jit(solution)/shard_map/all_to_all | solution.py:12
  158.1 11.0 %all_to_all.43 = bf16[8,48,256]{2,1,0:T(8,128)(2,1)S(1)} all-to-all(bf16[8,48,256]{2,1,0:T(8,128)(2,1)S(1)} %broadcast_in_dim.11), channel_id=1, replica_groups=mesh['y'=4,'x'=4,'z'=8,'c'=2] {'z'}, dimensions={0} | all-to-all | bytes 393216 | tf_op jit(solution)/shard_map/all_to_all | solution.py:12
  169.1 9.1 %collective-permute-start.4 = (bf16[384,256]{1,0:T(8,128)(2,1)S(1)}, bf16[384,256]{1,0:T(8,128)(2,1)S(1)}, u32[]{:S(2)}, u32[]{:S(2)}) collective-permute-start(bf16[384,256]{1,0:T(8,128)(2,1)S(1)} %bitcast.18), channel_id=1, source_target_pairs={{0,1},{1,0},{2,3},{3,2},{4,5},{5,4},{6,7},{7,6},{8,9},{9,8},{10,11... | collective-permute-start | bytes 589832 | tf_op jit(solution)/shard_map/ppermute | solution.py:21
  (45 shorter events, 8.3 us)
Async XLA Ops:
  0.0 4.9 %collective-permute-start = (bf16[256,1024]{1,0:T(8,128)(2,1)}, bf16[256,1024]{1,0:T(8,128)(2,1)S(1)}, u32[]{:S(2)}, u32[]{:S(2)}) collective-permute-start(bf16[256,1024]{1,0:T(8,128)(2,1)} %param.9), channel_id=1, source_target_pairs={{0,1},{1,0},{2,3},{3,2},{4,5},{5,4},{6,7},{7,6},{8,9},{9,8},{10,11... | collective-permute-start | bytes 1572872 | tf_op jit(solution)/shard_map/ppermute | solution.py:21
  37.0 3.9 %copy-start.4 = (bf16[1024,256]{1,0:T(8,128)(2,1)S(1)}, bf16[1024,256]{1,0:T(8,128)(2,1)}, u32[]{:S(2)}) copy-start(bf16[1024,256]{1,0:T(8,128)(2,1)} %param.10) | copy-start | bytes 1572868
  37.1 24.8 %all-to-all-start.1 = ((bf16[16,24,2048]{2,1,0:T(8,128)(2,1)}), bf16[16,24,2048]{2,1,0:T(8,128)(2,1)S(1)}, u32[]{:S(2)}, u32[]{:S(2)}) async-start(bf16[16,24,2048]{2,1,0:T(8,128)(2,1)} %broadcast_in_dim.8), calls=%async_computation.1 | async-start | bytes 3145728 | tf_op jit(solution)/shard_map/all_to_all | solution.py:12
  40.9 3.4 %collective-permute-start.1 = (bf16[1024,256]{1,0:T(8,128)(2,1)S(1)}, bf16[1024,256]{1,0:T(8,128)(2,1)S(1)}, u32[]{:S(2)}, u32[]{:S(2)}) collective-permute-start(bf16[1024,256]{1,0:T(8,128)(2,1)S(1)} %copy-done.4), channel_id=1, source_target_pairs={{0,1},{1,0},{2,3},{3,2},{4,5},{5,4},{6,7},{7,6},{8,9},{9,8},{10,11... | collective-permute-start | bytes 1572872 | tf_op jit(solution)/shard_map/ppermute | solution.py:21
  61.8 9.6 %copy-start.2 = (bf16[768,256]{1,0:T(8,128)(2,1)S(1)}, bf16[768,256]{1,0:T(8,128)(2,1)}, u32[]{:S(2)}) copy-start(bf16[768,256]{1,0:T(8,128)(2,1)} %param.7) | copy-start | bytes 1179652
  63.1 21.1 %copy-start.1 = (bf16[256,1024]{1,0:T(8,128)(2,1)S(1)}, bf16[256,1024]{1,0:T(8,128)(2,1)}, u32[]{:S(2)}) copy-start(bf16[256,1024]{1,0:T(8,128)(2,1)} %param.12) | copy-start | bytes 1572868
  63.1 30.3 %copy-start.3 = (f32[256]{0:T(256)S(1)}, f32[256]{0:T(256)}, u32[]{:S(2)}) copy-start(f32[256]{0:T(256)} %param.11) | copy-start | bytes 3076
  63.1 17.0 %all-to-all-start.2 = ((bf16[8,48,256]{2,1,0:T(8,128)(2,1)}), bf16[8,48,256]{2,1,0:T(8,128)(2,1)S(1)}, u32[]{:S(2)}, u32[]{:S(2)}) async-start(bf16[8,48,256]{2,1,0:T(8,128)(2,1)} %bitcast.2), calls=%async_computation.2 | async-start | bytes 393216 | tf_op jit(solution)/shard_map/all_to_all | solution.py:12
  80.8 11.9 %all-to-all-start.3 = ((bf16[8,48,256]{2,1,0:T(8,128)(2,1)}), bf16[8,48,256]{2,1,0:T(8,128)(2,1)S(1)}, u32[]{:S(2)}, u32[]{:S(2)}) async-start(bf16[8,48,256]{2,1,0:T(8,128)(2,1)} %broadcast_in_dim.9), calls=%async_computation.3 | async-start | bytes 393216 | tf_op jit(solution)/shard_map/all_to_all | solution.py:12
  84.2 9.2 %collective-permute-start.2 = (bf16[256,1024]{1,0:T(8,128)(2,1)S(1)}, bf16[256,1024]{1,0:T(8,128)(2,1)S(1)}, u32[]{:S(2)}, u32[]{:S(2)}) collective-permute-start(bf16[256,1024]{1,0:T(8,128)(2,1)S(1)} %copy-done.1), channel_id=1, source_target_pairs={{0,1},{1,0},{2,3},{3,2},{4,5},{5,4},{6,7},{7,6},{8,9},{9,8},{10,11... | collective-permute-start | bytes 1572872 | tf_op jit(solution)/shard_map/ppermute | solution.py:21
  93.4 0.7 copy-start
  123.2 3.9 %copy-start.5 = (bf16[1024,256]{1,0:T(8,128)(2,1)S(1)}, bf16[1024,256]{1,0:T(8,128)(2,1)}, u32[]{:S(2)}) copy-start(bf16[1024,256]{1,0:T(8,128)(2,1)} %param.13) | copy-start | bytes 1572868
  123.2 22.4 %all-to-all-start.5 = ((bf16[16,24,2048]{2,1,0:T(8,128)(2,1)}), bf16[16,24,2048]{2,1,0:T(8,128)(2,1)S(1)}, u32[]{:S(2)}, u32[]{:S(2)}) async-start(bf16[16,24,2048]{2,1,0:T(8,128)(2,1)} %broadcast_in_dim.10), calls=%async_computation.5 | async-start | bytes 3145728 | tf_op jit(solution)/shard_map/all_to_all | solution.py:12
  127.1 6.3 %collective-permute-start.3 = (bf16[1024,256]{1,0:T(8,128)(2,1)S(1)}, bf16[1024,256]{1,0:T(8,128)(2,1)S(1)}, u32[]{:S(2)}, u32[]{:S(2)}) collective-permute-start(bf16[1024,256]{1,0:T(8,128)(2,1)S(1)} %copy-done.5), channel_id=1, source_target_pairs={{0,1},{1,0},{2,3},{3,2},{4,5},{5,4},{6,7},{7,6},{8,9},{9,8},{10,11... | collective-permute-start | bytes 1572872 | tf_op jit(solution)/shard_map/ppermute | solution.py:21
  169.1 10.2 %collective-permute-start.4 = (bf16[384,256]{1,0:T(8,128)(2,1)S(1)}, bf16[384,256]{1,0:T(8,128)(2,1)S(1)}, u32[]{:S(2)}, u32[]{:S(2)}) collective-permute-start(bf16[384,256]{1,0:T(8,128)(2,1)S(1)} %bitcast.18), channel_id=1, source_target_pairs={{0,1},{1,0},{2,3},{3,2},{4,5},{5,4},{6,7},{7,6},{8,9},{9,8},{10,11... | collective-permute-start | bytes 589832 | tf_op jit(solution)/shard_map/ppermute | solution.py:21
